TPU v7x, 256 devices: a whole 4x4x8 slice. The times are simulated.
256 devices in a mesh: sp: 16 (over y, x), tp: 16 (over z, core).
Axes of the slice: x: 4, y: 4, z: 8, core: 2. Of those that a mesh axis runs over, the one named last changes fastest.
Arguments:
- latent: bfloat16 [8192, 4096], P(('sp', 'tp')), may hold values from -6 to 6
- context: bfloat16 [512, 4096], P('sp'), may hold values from -6 to 6
- condition: float32 [4096], replicated, may hold values from -6 to 6
- context_condition: float32 [4096], replicated, may hold values from -6 to 6
- modulation: bfloat16 [3, 4096, 4096], P(None, 'sp', 'tp'), may hold values from -0.09375 to 0.09375
- query_weight: bfloat16 [4096, 4096], P(None, 'tp'), as said below
- key_weight: bfloat16 [4096, 4096], P(None, 'tp'), as said below
- value_weight: bfloat16 [4096, 4096], P(None, 'tp'), may hold values from -0.09375 to 0.09375
- lambdas: float32 [16], P('tp'), may hold values from 0.3 to 0.8
- context_lift: float32 [16], P('tp'), may hold values from 1.5 to 3
- head_gain: float32 [256], replicated, may hold values from 0.1 to 1.9
- output_weight: bfloat16 [4096, 4096], P('tp'), may hold values from -0.09375 to 0.09375
Outputs:
- result: bfloat16 [8192, 4096], P(('sp', 'tp'))
Inputs may be any that keep to these rules, and one draw needn't show every extreme that they name: `query_weight`: entries lie within 200 / sqrt(4096) in magnitude. `key_weight`: entries lie within 6 / sqrt(4096) in magnitude.
All inputs are finite; a program needn't handle non-finite values.
Results may differ from a plain program's by a relative error of at most 0.025.
Values may be sent and summed in bfloat16 or wider, within the bound.
A program may use at most 64 MiB of HBM per device.

v0:
```python
import functools
import math
import jax
import jax.numpy as jnp
from jax import lax
from jax.sharding import Mesh
from jax.sharding import PartitionSpec as P

GRID_W = 64
SP = ("sp_0", "sp_1")
SP_TP = ("sp_0", "sp_1", "tp")
ROPE_BASE = 10000.0
EPSILON = 1e-05


def by_axis(shard, axes):
    return functools.reduce(lax.psum, axes, shard)


def from_everyone(shard, axis):
    copies = jnp.broadcast_to(shard, (lax.axis_size(axis), *shard.shape))
    return lax.all_to_all(copies, axis, split_axis=0, concat_axis=0, tiled=True)


def laid_out(pieces, dim):
    pieces = jnp.moveaxis(pieces, 0, dim)
    lengths = pieces.shape
    return pieces.reshape(*lengths[:dim], lengths[dim] * lengths[dim + 1], *lengths[dim + 2 :])


def collect(shard, axis, dim):
    pieces = from_everyone(shard, axis)
    return laid_out(pieces, dim)


def modulate(tokens_in, offset, scaling):
    values = tokens_in.astype(jnp.float32)
    center = jnp.mean(values, axis=-1, keepdims=True)
    spread = jnp.mean(jnp.square(values - center), axis=-1, keepdims=True)
    normed = (values - center) * lax.rsqrt(spread + EPSILON)
    return (normed * (1.0 + scaling) + offset).astype(jnp.bfloat16)


def rotate(tensor, places):
    number, head_count, head_width = tensor.shape
    quarter = head_width // 4
    eighth = head_width // 8
    inverse = ROPE_BASE ** (-jnp.arange(eighth, dtype=jnp.float32) / eighth)
    grid_row = (places // GRID_W).astype(jnp.float32)
    grid_col = (places % GRID_W).astype(jnp.float32)
    angles = jnp.stack([grid_row[:, None] * inverse, grid_col[:, None] * inverse], axis=1)
    cosine = jnp.cos(angles)[:, None, None, :, :]
    sine_table = jnp.sin(angles)[:, None, None, :, :]
    pieces = tensor.reshape(number, head_count, 2, 2, quarter)
    first_half = pieces[..., :eighth]
    second = pieces[..., eighth:]
    turned = jnp.concatenate(
        [first_half * cosine - second * sine_table, second * cosine + first_half * sine_table],
        axis=-1,
    )
    return turned.reshape(number, head_count, head_width)


def absorb(state_in, key_block, queries, lift_term, scale_factor):
    running_max, running_sum, running_out = state_in
    key_count = key_block.shape[0]
    head_count = queries.shape[1]
    head_width = 2 * queries.shape[3]
    local_width = head_count * head_width
    key_part = key_block[:, :local_width].reshape(key_count, head_count, 2, head_width // 2)
    value_part = key_block[:, local_width:].reshape(key_count, head_count, head_width)
    scores = (
        jnp.einsum("qhmd,khmd->mqhk", queries, key_part, preferred_element_type=jnp.float32)
        * scale_factor
        + lift_term
    )
    new_max = jnp.maximum(running_max, jnp.max(scores, axis=-1))
    fading = jnp.exp(running_max - new_max)
    weights = jnp.exp(scores - new_max[..., None])
    new_sum = running_sum * fading + jnp.sum(weights, axis=-1)
    new_out = running_out * fading[..., None] + jnp.einsum(
        "mqhk,khd->mqhd",
        weights.astype(jnp.bfloat16),
        value_part,
        preferred_element_type=jnp.float32,
    )
    return (new_max, new_sum, new_out)


def shards(
    latent,
    context,
    condition,
    context_condition,
    modulation,
    query_weight,
    key_weight,
    value_weight,
    lambdas,
    context_lift,
    head_gain,
    output_weight,
):
    sp_index = lax.axis_index(SP)
    rows_block = modulation.shape[1]
    silu_pair = jax.nn.silu(jnp.stack([condition, context_condition])).astype(jnp.bfloat16)
    own_rows = lax.dynamic_slice_in_dim(silu_pair, sp_index * rows_block, rows_block, 1)
    partial_mod = jnp.einsum(
        "cd,rde->cre", own_rows, modulation, preferred_element_type=jnp.float32
    )
    summed = by_axis(partial_mod, SP)
    mod_vectors = collect(summed, "tp", 2)
    head_count = lambdas.shape[0]
    head_width = query_weight.shape[1] // head_count
    half_width = head_width // 2
    local_width = head_count * head_width
    scale_factor = half_width ** (-0.5)
    normed = modulate(latent, mod_vectors[0, 0], mod_vectors[0, 1])
    projection = jnp.concatenate([query_weight, key_weight, value_weight], axis=1)
    projected = jnp.dot(
        lax.all_gather(normed, "tp", axis=0, tiled=True),
        projection,
        preferred_element_type=jnp.float32,
    ).astype(jnp.bfloat16)
    block_tokens = projected.shape[0]
    places = sp_index * block_tokens + jnp.arange(block_tokens, dtype=jnp.int32)
    queries = rotate(
        projected[:, :local_width]
        .astype(jnp.float32)
        .reshape(block_tokens, head_count, head_width),
        places,
    )
    queries = queries.astype(jnp.bfloat16).reshape(block_tokens, head_count, 2, half_width)
    latent_keys = rotate(
        projected[:, local_width : 2 * local_width]
        .astype(jnp.float32)
        .reshape(block_tokens, head_count, head_width),
        places,
    )
    latent_keys = latent_keys.astype(jnp.bfloat16).reshape(block_tokens, local_width)
    packed = jnp.concatenate([latent_keys, projected[:, 2 * local_width :]], axis=1)
    normed_context = modulate(context, mod_vectors[1, 0], mod_vectors[1, 1])
    own_context = jnp.dot(
        normed_context, projection[:, local_width:], preferred_element_type=jnp.float32
    ).astype(jnp.bfloat16)
    context_packed = collect(own_context, SP, 0)
    initial = (
        jnp.full((2, block_tokens, head_count), -jnp.inf, jnp.float32),
        jnp.zeros((2, block_tokens, head_count), jnp.float32),
        jnp.zeros((2, block_tokens, head_count, head_width), jnp.float32),
    )
    state_now = absorb(initial, context_packed, queries, context_lift[:, None], scale_factor)
    segment = lax.all_gather(packed, SP, axis=0, tiled=True)
    length = segment.shape[0]
    block_len = math.gcd(length, 1024)
    stacked = segment.reshape(length // block_len, block_len, segment.shape[1])

    def one_block(state_step, block_rows):
        return (absorb(state_step, block_rows, queries, 0.0, scale_factor), None)

    running_max, running_sum, running_out = lax.scan(one_block, state_now, stacked)[0]
    means = running_out / running_sum[..., None]
    difference = means[0] - lambdas[None, :, None] * means[1]
    scaled = (
        difference
        * lax.rsqrt(jnp.mean(jnp.square(difference), axis=-1, keepdims=True) + EPSILON)
        * head_gain
    )
    attended = scaled.astype(jnp.bfloat16).reshape(block_tokens, local_width)
    mixture = lax.psum_scatter(
        jnp.dot(attended, output_weight, preferred_element_type=jnp.float32).astype(jnp.bfloat16),
        "tp",
        scatter_dimension=0,
        tiled=True,
    ).astype(jnp.float32)
    return (latent.astype(jnp.float32) + mod_vectors[0, 2] * mixture).astype(jnp.bfloat16)


def solution(mesh):
    split = Mesh(mesh.devices.reshape(4, 4, mesh.shape["tp"]), ("sp_0", "sp_1", "tp"))
    return jax.shard_map(
        shards,
        mesh=split,
        in_specs=(
            P(SP_TP, None),
            P(SP, None),
            P(),
            P(),
            P(None, SP, "tp"),
            P(None, "tp"),
            P(None, "tp"),
            P(None, "tp"),
            P("tp"),
            P("tp"),
            P(),
            P("tp", None),
        ),
        out_specs=P(SP_TP, None),
        check_vma=False,
    )
```

profile of v0, /device:TPU:14, one launch (start us, length us, event | category | flops | bytes accessed | tf_op | source)
XLA Modules:
  0.0 305.2 jit_solution(5398257934742290326)
XLA Ops:
  6.5 1.4 fusion.78
  7.9 8.8 %psum.14 = f32[2,3,256]{2,0,1:T(2,128)S(1)} all-reduce(f32[2,3,256]{2,0,1:T(2,128)S(1)} %fusion.78), channel_id=1, replica_groups=mesh['sp_0'=4,'sp_1'=4,'tp'=16] {'sp_0'}, use_global_device_ids=true, to_apply=%region_0.1 | all-reduce | flops 1536 | bytes 12288 | tf_op jit(solution)/shard_map/psum | solution.py:17
  16.7 8.3 %psum.15 = f32[2,3,256]{2,0,1:T(2,128)S(1)} all-reduce(f32[2,3,256]{2,0,1:T(2,128)S(1)} %psum.14), channel_id=1, replica_groups=mesh['sp_0'=4,'sp_1'=4,'tp'=16] {'sp_1'}, use_global_device_ids=true, to_apply=%region_1.2 | all-reduce | flops 1536 | bytes 12288 | tf_op jit(solution)/shard_map/psum | solution.py:17
  25.7 7.9 %all-to-all-start = ((f32[16,2,3,256]{3,1,2,0:T(2,128)}), f32[16,2,3,256]{3,1,2,0:T(2,128)S(1)}, u32[]{:S(2)}, u32[]{:S(2)}) async-start(f32[16,2,3,256]{3,1,2,0:T(2,128)} %broadcast_in_dim.12), calls=%async_computation | async-start | bytes 196608 | tf_op jit(solution)/shard_map/all_to_all | solution.py:22
  35.9 6.0 %all-to-all-done = f32[16,2,3,256]{3,1,2,0:T(2,128)S(1)} async-done(((f32[16,2,3,256]{3,1,2,0:T(2,128)}), f32[16,2,3,256]{3,1,2,0:T(2,128)S(1)}, u32[]{:S(2)}, u32[]{:S(2)}) %all-to-all-start) | async-done | bytes 98336 | tf_op jit(solution)/shard_map/all_to_all | solution.py:22
  42.0 1.8 fusion.51
  44.4 38.9 %all-gather.3.cloned.1.call-done = bf16[512,4096]{1,0:T(8,128)(2,1)} async-done(((bf16[32,4096]{1,0:T(8,128)(2,1)}), bf16[512,4096]{1,0:T(8,128)(2,1)}) %all-gather.3.cloned.1.call-update) | async-done | bytes 4194320 | tf_op jit(solution)/shard_map/all_gather | solution.py:121
  83.4 7.5 %fusion.31 = bf16[512,768]{1,0:T(8,128)(2,1)S(1)} fusion(bf16[512,4096]{1,0:T(8,128)(2,1)} %all-gather.3.cloned.1.call-done, bf16[4096,256]{1,0:T(8,128)(2,1)} %param.21, bf16[4096,256]{1,0:T(8,128)(2,1)} %param.20, bf16[4096,256]{1,0:T(8,128)(2,1)} %param.19), kind=kOutput, calls=%fused_computation.37 | convolution fusion | flops 3240493056 | bytes 11272192 | tf_op jit(solution)/shard_map/dot_general | solution.py:120
  93.3 1.8 pad_maximum_fusion
  97.5 3.2 %fusion.36 = bf16[32,512]{1,0:T(8,128)(2,1)S(1)} fusion(bf16[4096,256]{1,0:T(8,128)(2,1)} %param.21, bf16[4096,256]{1,0:T(8,128)(2,1)} %param.20, bf16[32,4096]{1,0:T(8,128)(2,1)} %param.15, f32[4096]{0:T(1024)S(1)} %bitcast.171, f32[4096]{0:T(1024)S(1)} %bitcast.172, f32[32]{0:T(128)S(1)} %add_rsqrt_fusion.2, f32[32]{0:T(128)S(1)} %broadcast_multiply_fusion.3), kind=kOutput, calls=%fused_computation.41 | convolution fusion | flops 143409152 | bytes 4522240 | tf_op jit(solution)/shard_map/dot_general | solution.py:143
  101.6 7.2 %all-to-all-start.1 = ((bf16[16,32,512]{2,1,0:T(8,128)(2,1)}), bf16[16,32,512]{2,1,0:T(8,128)(2,1)S(1)}, u32[]{:S(2)}, u32[]{:S(2)}) async-start(bf16[16,32,512]{2,1,0:T(8,128)(2,1)} %broadcast_in_dim.13), calls=%async_computation.1 | async-start | bytes 1048576 | tf_op jit(solution)/shard_map/all_to_all | solution.py:22
  110.3 11.8 %all-to-all-done.1 = bf16[16,32,512]{2,1,0:T(8,128)(2,1)S(1)} async-done(((bf16[16,32,512]{2,1,0:T(8,128)(2,1)}), bf16[16,32,512]{2,1,0:T(8,128)(2,1)S(1)}, u32[]{:S(2)}, u32[]{:S(2)}) %all-to-all-start.1) | async-done | bytes 524320 | tf_op jit(solution)/shard_map/all_to_all | solution.py:22
  122.9 1.8 copy.35
  125.2 1.5 bitcast_reduce_fusion.1
  127.1 1.7 fusion.35
  128.9 43.7 %all-gather.5.cloned.1.call-done = bf16[8192,512]{1,0:T(8,128)(2,1)} async-done(((bf16[512,512]{1,0:T(8,128)(2,1)}), bf16[8192,512]{1,0:T(8,128)(2,1)}) %all-gather.5.cloned.1.call-update) | async-done | bytes 8388624 | tf_op jit(solution)/shard_map/all_gather | solution.py:153
  172.6 54.9 %while.14 = (s32[]{:T(128)}, f32[2,512,1]{1,0,2:T(2,128)S(1)}, f32[2,512,1]{1,0,2:T(2,128)S(1)}, f32[2,512,1,256]{1,3,0,2:T(8,128)}, bf16[8,1024,512]{2,1,0:T(8,...) while((s32[]{:T(128)}, f32[2,512,1]{1,0,2:T(2,128)S(1)}, f32[2,512,1]{1,0,2:T(2,128)S(1)}, ...), condition=%wide.region_11.12_spmd, body=%wide.region_8.11_spmd.sunk | while | flops 814222336 | bytes 33882276 | solution.py:161
  173.9 1.3 copy.54
  180.7 1.3 copy.54
  187.6 1.3 copy.54
  227.5 1.4 broadcast_divide_fusion
  229.0 3.3 %convolution_convert_fusion = bf16[512,4096]{1,0:T(8,128)(2,1)} fusion(bf16[256,4096]{1,0:T(8,128)(2,1)S(1)} %copy-done, f32[256]{0:T(256)S(1)} %copy-done.7, f32[512]{0:T(512)S(1)} %add_rsqrt_fusion, f32[2,512,1,256]{1,3,0,2:T(8,128)S(1)} %broadcast_divide_fusion, f32[]{:T(128)} %bitcast.145), kind=kOutput, calls=%fused_computation.26 | convolution fusion | flops 1076494336 | bytes 7343108 | tf_op jit(solution)/shard_map/dot_general | solution.py:171
  232.3 64.6 %reduce-scatter.2.cloned.1.call-done = bf16[32,4096]{1,0:T(8,128)(2,1)} async-done(((bf16[512,4096]{1,0:T(8,128)(2,1)}), bf16[32,4096]{1,0:T(8,128)(2,1)}) %reduce-scatter.2.cloned.1.call-update) | async-done | bytes 262160 | tf_op jit(solution)/shard_map/reduce_scatter | solution.py:170
  296.9 1.7 fusion.56
  (164 shorter events, 62.0 us)
Async XLA Ops:
  6.5 222.5 %copy-start = (bf16[256,4096]{1,0:T(8,128)(2,1)S(1)}, bf16[256,4096]{1,0:T(8,128)(2,1)}, u32[]{:S(2)}) copy-start(bf16[256,4096]{1,0:T(8,128)(2,1)} %param.25) | copy-start | bytes 6291460
  25.7 16.2 %all-to-all-start = ((f32[16,2,3,256]{3,1,2,0:T(2,128)}), f32[16,2,3,256]{3,1,2,0:T(2,128)S(1)}, u32[]{:S(2)}, u32[]{:S(2)}) async-start(f32[16,2,3,256]{3,1,2,0:T(2,128)} %broadcast_in_dim.12), calls=%async_computation | async-start | bytes 196608 | tf_op jit(solution)/shard_map/all_to_all | solution.py:22
  33.6 49.8 %all-gather.3.cloned.1.call-start = ((), (), s32[]{:S(2)}) async-start(), calls=%async_computation.3 | async-start | bytes 4456448 | tf_op jit(solution)/shard_map/all_gather | solution.py:121
  43.8 128.8 %all-gather.5.cloned.1.call-start = ((), (), s32[]{:S(2)}) async-start(), calls=%async_computation.4 | async-start | bytes 8912896 | tf_op jit(solution)/shard_map/all_gather | solution.py:153
  101.6 20.5 %all-to-all-start.1 = ((bf16[16,32,512]{2,1,0:T(8,128)(2,1)}), bf16[16,32,512]{2,1,0:T(8,128)(2,1)S(1)}, u32[]{:S(2)}, u32[]{:S(2)}) async-start(bf16[16,32,512]{2,1,0:T(8,128)(2,1)} %broadcast_in_dim.13), calls=%async_computation.1 | async-start | bytes 1048576 | tf_op jit(solution)/shard_map/all_to_all | solution.py:22
  108.8 188.1 %reduce-scatter.2.cloned.1.call-start = ((), (), s32[]{:S(2)}) async-start(), calls=%async_computation.5 | async-start | bytes 4456448 | tf_op jit(solution)/shard_map/reduce_scatter | solution.py:170
  122.1 2.6 copy-start.5
  125.0 2.1 copy-start.6
  172.6 56.4 %copy-start.7 = (f32[256]{0:T(256)S(1)}, f32[256]{0:T(256)}, u32[]{:S(2)}) copy-start(f32[256]{0:T(256)} %param.24) | copy-start | bytes 3076
  175.2 2.0 copy-start.1
  175.2 2.0 copy-start.2
  182.1 2.0 copy-start.1
  182.1 2.0 copy-start.2
  188.9 2.0 copy-start.1
  188.9 2.0 copy-start.2
  195.8 2.0 copy-start.2
  202.6 2.0 copy-start.2
  209.5 2.0 copy-start.1
  209.5 2.0 copy-start.2
  216.4 2.0 copy-start.1
  216.4 2.0 copy-start.2
  223.2 2.0 copy-start.1
  223.2 2.0 copy-start.2
  229.0 67.9 %copy-start.4 = (bf16[32,4096]{1,0:T(8,128)(2,1)S(1)}, bf16[32,4096]{1,0:T(8,128)(2,1)}, u32[]{:S(2)}) copy-start(bf16[32,4096]{1,0:T(8,128)(2,1)} %param.14) | copy-start | bytes 786436
  (10 other events, 12.6 us)
Sparse Core Ops, SparseCore 0:
  43.9 39.4 all-gather.2
  95.3 77.2 all-gather.4
  232.5 64.4 reduce-scatter.1
where the time goes:
time: 306 us; the launch traced here: 305 us
  waiting for transfers between devices  165 us (54%)
  local copies, waits for them, and re-layouts  39.2 us (13%)
  matrix products  33.8 us (11%)
  other arithmetic  19.6 us (6%)
  blocking collectives  17.1 us (6%)
  starting transfers between devices  15.4 us (5%)
  between operations  14.6 us (5%)
    reduce_scatter x1, waiting for transfers between devices, shards(): lax.psum_scatter(jnp.dot(attended, output_weight, preferred_element_type=...  64.6 us
    all_gather x1, waiting for transfers between devices, shards(): segment = lax.all_gather(packed, SP, axis=0, tiled=True)  43.7 us
    all_gather x1, waiting for transfers between devices, shards(): lax.all_gather(normed, 'tp', axis=0, tiled=True)  38.9 us
    dynamic_slice x16, local copies, waits for them, and re-layouts, shards(): lax.scan(one_block, state_now, stacked)[0]  20.8 us
    all_to_all x2, waiting for transfers between devices, from_everyone(): return lax.all_to_all(copies, axis, split_axis=0, concat_axis=0, tiled=True)  17.7 us
    psum x2, blocking collectives, by_axis(): return functools.reduce(lax.psum, axes, shard)  17.1 us
    all_to_all x2, starting transfers between devices, from_everyone(): return lax.all_to_all(copies, axis, split_axis=0, concat_axis=0, tiled=True)  15.1 us
    slice x10, local copies, waits for them, and re-layouts, absorb(): key_block[:, :local_width]  12.4 us
  transfers between devices with their start and end apart: 5, of which 5 were waited for; matrix products, arithmetic and copies ran while one was open for 5% of the time, Pallas kernels for 0%

commit v1 on v0

--- a/solution.py
+++ b/solution.py
@@ -11,6 +11,11 @@
 SP_TP = ("sp_0", "sp_1", "tp")
 ROPE_BASE = 10000.0
 EPSILON = 1e-05
+
+
+def exchange_gather(x, mesh_axis, dim):
+    sent = jnp.stack([x] * lax.axis_size(mesh_axis))
+    return jnp.concatenate(lax.all_to_all(sent, mesh_axis, 0, 0), axis=dim)
 
 
 def by_axis(shard, axes):
@@ -150,7 +155,7 @@
         jnp.zeros((2, block_tokens, head_count, head_width), jnp.float32),
     )
     state_now = absorb(initial, context_packed, queries, context_lift[:, None], scale_factor)
-    segment = lax.all_gather(packed, SP, axis=0, tiled=True)
+    segment = exchange_gather(packed, SP, 0)
     length = segment.shape[0]
     block_len = math.gcd(length, 1024)
     stacked = segment.reshape(length // block_len, block_len, segment.shape[1])

time: 306 us -> 361 us (1.18)
  waiting for transfers between devices: 165 us -> 206 us
  starting transfers between devices: 15.4 us -> 25 us
  local copies, waits for them, and re-layouts: 39.2 us -> 43.2 us
    all_to_all x0 -> x1, waiting for transfers between devices: none -> 113 us  [exchange_gather(): return jnp.concatenate(lax.all_to_all(sent, mesh_axis, 0, 0), axis=dim)]
    all_gather x1 -> x0, waiting for transfers between devices: 43.7 us -> none  [shards(): segment = lax.all_gather(packed, SP, axis=0, tiled=True)]
    all_gather x1, waiting for transfers between devices: 38.9 us -> 23 us  [shards(): lax.all_gather(normed, 'tp', axis=0, tiled=True)]
    all_to_all x2, waiting for transfers between devices: 17.7 us -> 5.95 us  [from_everyone(): return lax.all_to_all(copies, axis, split_axis=0, concat_axis=0, tiled=True)]
    all_to_all x0 -> x1, starting transfers between devices: none -> 7.24 us  [exchange_gather(): return jnp.concatenate(lax.all_to_all(sent, mesh_axis, 0, 0), axis=dim)]
    another operation x0 -> x1, local copies, waits for them, and re-layouts: none -> 4.02 us  [exchange_gather(): sent = jnp.stack([x] * lax.axis_size(mesh_axis))]
  transfers between devices with their start and end apart: 5 -> 5, of which waited for: 5 -> 4; matrix products, arithmetic and copies ran while one was open for 5% -> 8% of each run, Pallas kernels for 0% -> 0%
where the time goes in v1:
time: 361 us; the launch traced here: 360 us
  waiting for transfers between devices  206 us (57%)
  local copies, waits for them, and re-layouts  43.2 us (12%)
  matrix products  34.7 us (10%)
  starting transfers between devices  25 us (7%)
  other arithmetic  18.9 us (5%)
  blocking collectives  17.1 us (5%)
  between operations  14.9 us (4%)
    all_to_all x1, waiting for transfers between devices, exchange_gather(): return jnp.concatenate(lax.all_to_all(sent, mesh_axis, 0, 0), axis=dim)  113 us
    reduce_scatter x1, waiting for transfers between devices, shards(): lax.psum_scatter(jnp.dot(attended, output_weight, preferred_element_type=...  63.9 us
    all_gather x1, waiting for transfers between devices, shards(): lax.all_gather(normed, 'tp', axis=0, tiled=True)  23 us
    dynamic_slice x16, local copies, waits for them, and re-layouts, shards(): lax.scan(one_block, state_now, stacked)[0]  21.5 us
    all_to_all x2, starting transfers between devices, from_everyone(): return lax.all_to_all(copies, axis, split_axis=0, concat_axis=0, tiled=True)  17.5 us
    psum x2, blocking collectives, by_axis(): return functools.reduce(lax.psum, axes, shard)  17.1 us
    dot_general x9, matrix products, absorb(): jnp.einsum('mqhk,khd->mqhd', weights.astype(jnp.bfloat16), value_part, pr...  11.7 us
    slice x10, local copies, waits for them, and re-layouts, absorb(): key_block[:, :local_width]  11.6 us
  transfers between devices with their start and end apart: 5, of which 4 were waited for; matrix products, arithmetic and copies ran while one was open for 8% of the time, Pallas kernels for 0%

profile of v1, /device:TPU:14, one launch (start us, length us, event | category | flops | bytes accessed | tf_op | source)
XLA Modules:
  0.0 360.0 jit_solution(11918117705345531628)
XLA Ops:
  6.5 1.4 fusion.78
  7.9 8.8 %psum.14 = f32[2,3,256]{2,0,1:T(2,128)S(1)} all-reduce(f32[2,3,256]{2,0,1:T(2,128)S(1)} %fusion.78), channel_id=1, replica_groups=mesh['sp_0'=4,'sp_1'=4,'tp'=16] {'sp_0'}, use_global_device_ids=true, to_apply=%region_0.1 | all-reduce | flops 1536 | bytes 12288 | tf_op jit(solution)/shard_map/psum | solution.py:22
  16.7 8.3 %psum.15 = f32[2,3,256]{2,0,1:T(2,128)S(1)} all-reduce(f32[2,3,256]{2,0,1:T(2,128)S(1)} %psum.14), channel_id=1, replica_groups=mesh['sp_0'=4,'sp_1'=4,'tp'=16] {'sp_1'}, use_global_device_ids=true, to_apply=%region_1.2 | all-reduce | flops 1536 | bytes 12288 | tf_op jit(solution)/shard_map/psum | solution.py:22
  25.7 7.9 %all-to-all-start = ((f32[16,2,3,256]{3,1,2,0:T(2,128)}), f32[16,2,3,256]{3,1,2,0:T(2,128)S(1)}, u32[]{:S(2)}, u32[]{:S(2)}) async-start(f32[16,2,3,256]{3,1,2,0:T(2,128)} %broadcast_in_dim.12), calls=%async_computation | async-start | bytes 196608 | tf_op jit(solution)/shard_map/all_to_all | solution.py:27
  35.9 6.0 %all-to-all-done = f32[16,2,3,256]{3,1,2,0:T(2,128)S(1)} async-done(((f32[16,2,3,256]{3,1,2,0:T(2,128)}), f32[16,2,3,256]{3,1,2,0:T(2,128)S(1)}, u32[]{:S(2)}, u32[]{:S(2)}) %all-to-all-start) | async-done | bytes 98336 | tf_op jit(solution)/shard_map/all_to_all | solution.py:27
  42.0 1.8 fusion.51
  46.7 3.2 fusion.36
  50.7 9.6 %all-to-all-start.1 = ((bf16[16,32,512]{2,1,0:T(8,128)(2,1)}), bf16[16,32,512]{2,1,0:T(8,128)(2,1)}, u32[]{:S(2)}, u32[]{:S(2)}) async-start(bf16[16,32,512]{2,1,0:T(8,128)(2,1)} %broadcast_in_dim.13), calls=%async_computation.1 | async-start | bytes 1048576 | tf_op jit(solution)/shard_map/all_to_all | solution.py:27
  60.4 23.0 %all-gather.2.cloned.1.call-done = bf16[512,4096]{1,0:T(8,128)(2,1)} async-done(((bf16[32,4096]{1,0:T(8,128)(2,1)}), bf16[512,4096]{1,0:T(8,128)(2,1)}) %all-gather.2.cloned.1.call-update) | async-done | bytes 4194320 | tf_op jit(solution)/shard_map/all_gather | solution.py:126
  83.4 7.5 %fusion.31 = bf16[512,768]{1,0:T(8,128)(2,1)S(1)} fusion(bf16[512,4096]{1,0:T(8,128)(2,1)} %all-gather.2.cloned.1.call-done, bf16[4096,256]{1,0:T(8,128)(2,1)} %param.21, bf16[4096,256]{1,0:T(8,128)(2,1)} %param.20, bf16[4096,256]{1,0:T(8,128)(2,1)} %param.19), kind=kOutput, calls=%fused_computation.37 | convolution fusion | flops 3240493056 | bytes 11272192 | tf_op jit(solution)/shard_map/dot_general | solution.py:125
  95.1 4.0 %stack.14 = bf16[16,512,512]{2,1,0:T(8,128)(2,1)} broadcast(bf16[512,512]{1,0:T(8,128)(2,1)S(1)} %pad_maximum_fusion), dimensions={1,2} | broadcast | bytes 8912896 | tf_op jit(solution)/shard_map/stack | solution.py:17
  99.1 7.2 %all-to-all-start.2 = ((bf16[16,512,512]{2,1,0:T(8,128)(2,1)}), bf16[16,512,512]{2,1,0:T(8,128)(2,1)}, u32[]{:S(2)}, u32[]{:S(2)}) async-start(bf16[16,512,512]{2,1,0:T(8,128)(2,1)} %stack.14), calls=%async_computation.2 | async-start | bytes 16777216 | tf_op jit(solution)/shard_map/all_to_all | solution.py:18
  110.2 1.5 bitcast_reduce_fusion.1
  112.1 2.6 fusion.35
  114.8 112.9 %all-to-all-done.2 = bf16[16,512,512]{2,1,0:T(8,128)(2,1)} async-done(((bf16[16,512,512]{2,1,0:T(8,128)(2,1)}), bf16[16,512,512]{2,1,0:T(8,128)(2,1)}, u32[]{:S(2)}, u32[]{:S(2)}) %all-to-all-start.2) | async-done | bytes 8388640 | tf_op jit(solution)/shard_map/all_to_all | solution.py:18
  227.6 55.0 %while.14 = (s32[]{:T(128)}, f32[2,512,1]{1,0,2:T(2,128)S(1)}, f32[2,512,1]{1,0,2:T(2,128)S(1)}, f32[2,512,1,256]{1,3,0,2:T(8,128)}, bf16[8,1024,512]{2,1,0:T(8,...) while((s32[]{:T(128)}, f32[2,512,1]{1,0,2:T(2,128)S(1)}, f32[2,512,1]{1,0,2:T(2,128)S(1)}, ...), condition=%wide.region_11.12_spmd, body=%wide.region_8.11_spmd.sunk | while | flops 814222336 | bytes 33882276 | solution.py:166
  228.9 1.4 copy.53
  235.8 1.4 copy.53
  242.7 1.4 copy.53
  249.5 1.4 copy.53
  277.0 1.4 copy.53
  284.1 3.3 convolution_convert_fusion
  287.5 63.9 %reduce-scatter.2.cloned.1.call-done = bf16[32,4096]{1,0:T(8,128)(2,1)} async-done(((bf16[512,4096]{1,0:T(8,128)(2,1)}), bf16[32,4096]{1,0:T(8,128)(2,1)}) %reduce-scatter.2.cloned.1.call-update) | async-done | bytes 262160 | tf_op jit(solution)/shard_map/reduce_scatter | solution.py:175
  351.4 1.7 fusion.56
  (160 shorter events, 63.1 us)
Async XLA Ops:
  6.5 277.6 %copy-start = (bf16[256,4096]{1,0:T(8,128)(2,1)S(1)}, bf16[256,4096]{1,0:T(8,128)(2,1)}, u32[]{:S(2)}) copy-start(bf16[256,4096]{1,0:T(8,128)(2,1)} %param.25) | copy-start | bytes 6291460
  25.7 16.2 %all-to-all-start = ((f32[16,2,3,256]{3,1,2,0:T(2,128)}), f32[16,2,3,256]{3,1,2,0:T(2,128)S(1)}, u32[]{:S(2)}, u32[]{:S(2)}) async-start(f32[16,2,3,256]{3,1,2,0:T(2,128)} %broadcast_in_dim.12), calls=%async_computation | async-start | bytes 196608 | tf_op jit(solution)/shard_map/all_to_all | solution.py:27
  33.6 49.8 %all-gather.2.cloned.1.call-start = ((), (), s32[]{:S(2)}) async-start(), calls=%async_computation.4 | async-start | bytes 4456448 | tf_op jit(solution)/shard_map/all_gather | solution.py:126
  50.7 44.4 %all-to-all-start.1 = ((bf16[16,32,512]{2,1,0:T(8,128)(2,1)}), bf16[16,32,512]{2,1,0:T(8,128)(2,1)}, u32[]{:S(2)}, u32[]{:S(2)}) async-start(bf16[16,32,512]{2,1,0:T(8,128)(2,1)} %broadcast_in_dim.13), calls=%async_computation.1 | async-start | bytes 1048576 | tf_op jit(solution)/shard_map/all_to_all | solution.py:27
  99.1 128.5 %all-to-all-start.2 = ((bf16[16,512,512]{2,1,0:T(8,128)(2,1)}), bf16[16,512,512]{2,1,0:T(8,128)(2,1)}, u32[]{:S(2)}, u32[]{:S(2)}) async-start(bf16[16,512,512]{2,1,0:T(8,128)(2,1)} %stack.14), calls=%async_computation.2 | async-start | bytes 16777216 | tf_op jit(solution)/shard_map/all_to_all | solution.py:18
  106.4 245.0 %reduce-scatter.2.cloned.1.call-start = ((), (), s32[]{:S(2)}) async-start(), calls=%async_computation.5 | async-start | bytes 4456448 | tf_op jit(solution)/shard_map/reduce_scatter | solution.py:175
  227.6 56.5 %copy-start.5 = (f32[256]{0:T(256)S(1)}, f32[256]{0:T(256)}, u32[]{:S(2)}) copy-start(f32[256]{0:T(256)} %param.24) | copy-start | bytes 3076
  230.3 2.0 copy-start.1
  230.3 2.0 copy-start.2
  237.2 2.0 copy-start.1
  237.2 2.0 copy-start.2
  244.1 2.0 copy-start.1
  244.1 2.0 copy-start.2
  250.9 2.0 copy-start.1
  250.9 2.0 copy-start.2
  257.8 2.0 copy-start.1
  257.8 2.0 copy-start.2
  264.7 2.0 copy-start.1
  264.7 2.0 copy-start.2
  271.6 2.0 copy-start.1
  271.6 2.0 copy-start.2
  278.4 2.0 copy-start.1
  278.4 2.0 copy-start.2
  284.1 67.3 %copy-start.4 = (bf16[32,4096]{1,0:T(8,128)(2,1)S(1)}, bf16[32,4096]{1,0:T(8,128)(2,1)}, u32[]{:S(2)}) copy-start(bf16[32,4096]{1,0:T(8,128)(2,1)} %param.14) | copy-start | bytes 786436
  (8 other events, 8.0 us)
Sparse Core Ops, SparseCore 0:
  43.9 39.4 all-gather.1
  287.6 63.7 reduce-scatter.1
